TPU v7x, 512 devices: a whole 4x4x16 slice. The times are simulated.
512 devices in a mesh: ep: 16 (over y, x), tp: 32 (over z, core).
Axes of the slice: x: 4, y: 4, z: 16, core: 2. Of those that a mesh axis runs over, the one named last changes fastest.
Arguments:
- tokens: bfloat16 [2048, 4096], P('ep', 'tp'), may hold values from -16 to 16
- routing: int32 [2048, 4], P('ep'), may hold values from 0 to 31, all different within a row; in each aligned block of 128 rows (0 to 127, 128 to 255, ...) at most 32 rows name the same one
- gate_weights: float32 [2048, 4], P('ep'), may hold values from 0.1 to 1
- w_gate: bfloat16 [32, 1024, 4096], P('ep', 'tp'), may hold values from -0.09375 to 0.09375
- w_up: bfloat16 [32, 1024, 4096], P('ep', 'tp'), may hold values from -0.09375 to 0.09375
- w_down: bfloat16 [32, 1024, 4096], P('ep', None, 'tp'), may hold values from -2 to 2
- out_gain: float32 [4096], P('tp'), may hold values from 0.1 to 1.9
Outputs:
- mixed: bfloat16 [2048, 4096], P('ep', 'tp')
Inputs may be any that keep to these rules, and one draw needn't show every extreme that they name: `routing`: in each aligned block of 128 rows (the tokens of one index of ep) no expert is named by more than 32 entries, and in every draw some expert is named by exactly 32 entries of some block. The 4 entries of a row differ.
All inputs are finite; a program needn't handle non-finite values.
Results may differ from a plain program's by a relative error of at most 0.0057.
Values may be sent and summed in bfloat16 or wider, within the bound.
A program may use at most 64 MiB of HBM per device.

v0:
```python
import jax
import jax.numpy as jnp
from jax import lax
from jax.sharding import PartitionSpec as P

D = 4096
TOPK = 4
EXP_DEV = 2
norm_eps = 1e-05


def from_everyone(value, axis):
    length = lax.axis_size(axis)
    return lax.all_to_all(
        jnp.broadcast_to(value[None], (length, *value.shape)), axis, 0, 0, tiled=True
    )


def taken_together(value, axis):
    return from_everyone(value, axis).sum(axis=0)


def body(tokens, routing, gate_weights, w_gate, w_up, w_down, out_gain):
    ep_count = lax.axis_size("ep")
    tok_rows = tokens.shape[0]
    width_part = tokens.shape[1]
    experts = EXP_DEV * ep_count
    slot_count = 2 * tok_rows * TOPK // experts
    span_rows = ep_count * slot_count
    total_slots = EXP_DEV * span_rows
    flat_route = routing.reshape(-1)
    expert_ids = jnp.arange(experts, dtype=jnp.int32)
    hit_table = (flat_route[:, None] == expert_ids[None, :]).astype(jnp.int32)
    running = jnp.cumsum(hit_table, axis=0) - hit_table
    slot_rank = jnp.sum(running * hit_table, axis=1)
    slot_target = flat_route % EXP_DEV * span_rows + flat_route // EXP_DEV * slot_count + slot_rank
    entry_targets = slot_target.reshape(tok_rows, TOPK)
    slot_ids = jnp.arange(total_slots, dtype=jnp.int32)
    select_table = jnp.any(entry_targets[None, :, :] == slot_ids[:, None, None], axis=2).astype(
        jnp.bfloat16
    )
    outgoing = jnp.dot(select_table, tokens, preferred_element_type=jnp.float32).astype(
        jnp.bfloat16
    )
    outgoing = outgoing.reshape(EXP_DEV, ep_count, slot_count, width_part)
    arrived = lax.all_to_all(outgoing, "ep", split_axis=1, concat_axis=1, tiled=True).reshape(
        EXP_DEV, span_rows, width_part
    )
    piece_cols = lax.all_gather(arrived, "tp", axis=2, tiled=True)
    gate_sum = jnp.einsum("efn,esn->efs", w_gate, piece_cols, preferred_element_type=jnp.float32)
    up_sum = jnp.einsum("efn,esn->efs", w_up, piece_cols, preferred_element_type=jnp.float32)
    square_sum = jnp.einsum(
        "esn,esn->es", piece_cols, piece_cols, preferred_element_type=jnp.float32
    )
    row_scale = lax.rsqrt(square_sum / D + norm_eps)[:, None, :]
    hidden = (jax.nn.silu(gate_sum * row_scale) * (up_sum * row_scale)).astype(jnp.bfloat16)
    out_part = w_down.shape[2]
    expert_out = jnp.einsum(
        "ens,end->esd",
        lax.all_gather(hidden, "tp", axis=1, tiled=True),
        w_down,
        preferred_element_type=jnp.float32,
    ).astype(jnp.bfloat16)
    returned = lax.all_to_all(
        expert_out.reshape(EXP_DEV, ep_count, slot_count, out_part),
        "ep",
        split_axis=1,
        concat_axis=1,
        tiled=True,
    )
    returned = returned.reshape(total_slots, out_part)
    chosen = returned[slot_target].astype(jnp.float32).reshape(tok_rows, TOPK, out_part)
    combined = jnp.sum(chosen * gate_weights[:, :, None], axis=1)
    square_total = taken_together(jnp.sum(combined * combined, axis=1), "tp")
    final_scale = lax.rsqrt(square_total / D + norm_eps)
    return (combined * final_scale[:, None] * out_gain[None, :]).astype(jnp.bfloat16)


def solution(mesh):
    placed = (
        P("ep", "tp"),
        P("ep", None),
        P("ep", None),
        P("ep", "tp", None),
        P("ep", "tp", None),
        P("ep", None, "tp"),
        P("tp"),
    )
    return jax.shard_map(body, mesh=mesh, in_specs=placed, out_specs=P("ep", "tp"), check_vma=False)
```

profile of v0, /device:TPU:1, one launch (start us, length us, event | category | flops | bytes accessed | tf_op | source)
XLA Modules:
  0.0 253.4 jit_solution(5410838036807146994)
XLA Ops:
  6.5 0.0 copy-start
  6.5 0.0 copy-start.2
  6.5 0.0 all-gather.3.cloned.1.call-start
  6.5 0.9 copy.73
  7.4 0.1 eq.44
  7.5 0.1 eq.40
  7.6 1.2 reduce-window.6
  8.8 0.2 slice_reduce_fusion
  9.1 0.1 fusion.9
  9.2 0.1 reduce_sum.41
  9.3 0.1 copy.76
  9.4 0.7 fusion.13
  10.1 0.4 fusion.1
  10.4 1.0 convolution_convert_fusion.1
  11.5 14.9 %all_to_all.16 = bf16[2,16,32,128]{3,2,0,1:T(8,128)(2,1)S(1)} all-to-all(bf16[2,16,32,128]{3,2,0,1:T(8,128)(2,1)S(1)} %copy.77), channel_id=1, replica_groups=mesh['ep'=16,'tp'=32] {'ep'}, dimensions={1} | all-to-all | bytes 524288 | tf_op jit(solution)/shard_map/all_to_all | solution.py:46
  26.4 0.7 copy.78
  27.1 0.0 all-gather.3.cloned.1.call-update
  27.1 0.0 all-gather.5.cloned.1.call-start
  27.2 98.1 %all-gather.3.cloned.1.call-done = bf16[2,512,4096]{2,1,0:T(8,128)(2,1)} async-done(((bf16[2,512,128]{2,1,0:T(8,128)(2,1)}), bf16[2,512,4096]{2,1,0:T(8,128)(2,1)}) %all-gather.3.cloned.1.call-update) | async-done | bytes 8388624 | tf_op jit(solution)/shard_map/all_gather | solution.py:49
  125.2 0.0 copy-start.1
  125.2 0.0 copy-start.3
  125.2 5.2 %fusion = f32[2,512]{1,0:T(2,128)S(1)} fusion(bf16[2,512,4096]{2,1,0:T(8,128)(2,1)} %all-gather.3.cloned.1.call-done), kind=kLoop, calls=%fused_computation.2 | loop fusion | flops 12581888 | bytes 8392704 | tf_op jit(solution)/shard_map/esn,esn->es/dot_general | solution.py:52
  130.5 0.0 copy-done.2
  130.5 0.5 copy-done.1
  131.0 0.0 copy-start.4
  131.0 2.6 %fusion.3 = f32[2,32,512]{2,1,0:T(8,128)S(1)} fusion(bf16[2,512,4096]{2,1,0:T(8,128)(2,1)S(1)} %copy-done.1, bf16[2,32,4096]{2,1,0:T(8,128)(2,1)S(1)} %copy-done.2, f32[2,512]{1,0:T(2,128)S(1)} %add_rsqrt_fusion), kind=kOutput, calls=%fused_computation.10 | convolution fusion | flops 268468224 | bytes 9048064 | tf_op jit(solution)/shard_map/efn,esn->efs/dot_general | solution.py:50
  133.6 0.0 copy-done.3
  133.7 0.0 copy-start.5
  133.7 3.2 %fusion.5 = bf16[2,32,512]{2,1,0:T(8,128)(2,1)} fusion(bf16[2,512,4096]{2,1,0:T(8,128)(2,1)S(1)} %copy-done.1, bf16[2,32,4096]{2,1,0:T(8,128)(2,1)S(1)} %copy-done.3, f32[2,32,512]{2,1,0:T(8,128)S(1)} %fusion.3, f32[2,512]{1,0:T(2,128)S(1)} %add_rsqrt_fusion), kind=kOutput, calls=%fused_computation.12 | convolution fusion | flops 268664832 | bytes 9113600 | tf_op jit(solution)/shard_map/efn,esn->efs/dot_general | solution.py:51
  136.9 0.0 all-gather.5.cloned.1.call-update
  136.9 0.1 reshape.209
  137.0 0.0 copy-done.4
  137.0 0.1 copy.82
  137.2 67.7 %all-gather.5.cloned.1.call-done = bf16[2,1024,512]{2,1,0:T(8,128)(2,1)} async-done(((bf16[2,32,512]{2,1,0:T(8,128)(2,1)}), bf16[2,1024,512]{2,1,0:T(8,128)(2,1)}) %all-gather.5.cloned.1.call-update) | async-done | bytes 2097168 | tf_op jit(solution)/shard_map/all_gather | solution.py:60
  204.9 0.0 copy-done
  204.9 2.5 convolution_convert_fusion
  207.4 0.7 copy.79
  208.1 6.5 %all-to-all-start.1 = ((bf16[2,16,32,128]{3,2,0,1:T(8,128)(2,1)}), bf16[2,16,32,128]{3,2,0,1:T(8,128)(2,1)S(1)}, u32[]{:S(2)}, u32[]{:S(2)}) async-start(bf16[2,16,32,128]{3,2,0,1:T(8,128)(2,1)} %copy.79), calls=%async_computation.1 | async-start | bytes 524288 | tf_op jit(solution)/shard_map/all_to_all | solution.py:64
  214.7 8.2 %all-to-all-done.1 = bf16[2,16,32,128]{3,2,0,1:T(8,128)(2,1)S(1)} async-done(((bf16[2,16,32,128]{3,2,0,1:T(8,128)(2,1)}), bf16[2,16,32,128]{3,2,0,1:T(8,128)(2,1)S(1)}, u32[]{:S(2)}, u32[]{:S(2)}) %all-to-all-start.1) | async-done | bytes 262176 | tf_op jit(solution)/shard_map/all_to_all | solution.py:64
  222.9 1.3 gather_fusion
  224.2 0.2 fusion.6
  224.5 0.1 multiply_reduce_fusion
  224.6 21.2 %all_to_all.17 = f32[32,1,128]{2,1,0:T(1,128)S(1)} all-to-all(f32[32,1,128]{2,1,0:T(1,128)S(1)} %broadcast_in_dim.2), channel_id=1, replica_groups=mesh['ep'=16,'tp'=32] {'tp'}, dimensions={0} | all-to-all | bytes 32768 | tf_op jit(solution)/shard_map/all_to_all | solution.py:14
  245.9 0.0 copy-done.5
  245.9 0.7 multiply_convert_fusion
  (11 shorter events, 0.2 us)
Async XLA Ops:
  6.5 198.4 %copy-start = (bf16[2,1024,128]{2,1,0:T(8,128)(2,1)S(1)}, bf16[2,1024,128]{2,1,0:T(8,128)(2,1)}, u32[]{:S(2)}) copy-start(bf16[2,1024,128]{2,1,0:T(8,128)(2,1)} %param.12) | copy-start | bytes 1572868
  6.5 124.0 %copy-start.2 = (bf16[2,32,4096]{2,1,0:T(8,128)(2,1)S(1)}, bf16[2,32,4096]{2,1,0:T(8,128)(2,1)}, u32[]{:S(2)}) copy-start(bf16[2,32,4096]{2,1,0:T(8,128)(2,1)} %param.10) | copy-start | bytes 1572868
  6.5 118.7 %all-gather.3.cloned.1.call-start = ((), (), s32[]{:S(2)}) async-start(), calls=%async_computation.3 | async-start | bytes 8650752 | tf_op jit(solution)/shard_map/all_gather | solution.py:49
  27.1 177.8 %all-gather.5.cloned.1.call-start = ((), (), s32[]{:S(2)}) async-start(), calls=%async_computation.4 | async-start | bytes 2162688 | tf_op jit(solution)/shard_map/all_gather | solution.py:60
  125.2 5.8 %copy-start.1 = (bf16[2,512,4096]{2,1,0:T(8,128)(2,1)S(1)}, bf16[2,512,4096]{2,1,0:T(8,128)(2,1)}, u32[]{:S(2)}) copy-start(bf16[2,512,4096]{2,1,0:T(8,128)(2,1)} %all-gather.3.cloned.1.call-done) | copy-start | bytes 25165828
  125.2 8.4 %copy-start.3 = (bf16[2,32,4096]{2,1,0:T(8,128)(2,1)S(1)}, bf16[2,32,4096]{2,1,0:T(8,128)(2,1)}, u32[]{:S(2)}) copy-start(bf16[2,32,4096]{2,1,0:T(8,128)(2,1)} %param.11) | copy-start | bytes 1572868
  131.0 6.0 %copy-start.4 = (f32[128,4]{0,1:T(4,128)S(1)}, f32[128,4]{0,1:T(4,128)}, u32[]{:S(2)}) copy-start(f32[128,4]{0,1:T(4,128)} %param.9) | copy-start | bytes 6148
  133.7 112.2 %copy-start.5 = (f32[128]{0:T(128)S(1)}, f32[128]{0:T(128)}, u32[]{:S(2)}) copy-start(f32[128]{0:T(128)} %param.13) | copy-start | bytes 1540
  208.1 14.7 %all-to-all-start.1 = ((bf16[2,16,32,128]{3,2,0,1:T(8,128)(2,1)}), bf16[2,16,32,128]{3,2,0,1:T(8,128)(2,1)S(1)}, u32[]{:S(2)}, u32[]{:S(2)}) async-start(bf16[2,16,32,128]{3,2,0,1:T(8,128)(2,1)} %copy.79), calls=%async_computation.1 | async-start | bytes 524288 | tf_op jit(solution)/shard_map/all_to_all | solution.py:64
Sparse Core Ops, SparseCore 0:
  27.2 97.9 all-gather.2
  137.0 67.7 all-gather.4
where the time goes:
time: 254 us; the launch traced here: 253 us
  waiting for transfers between devices  174 us (69%)
  blocking collectives  36.1 us (14%)
  between operations  13.5 us (5%)
  matrix products  9.35 us (4%)
  other arithmetic  8.73 us (3%)
  starting transfers between devices  6.57 us (3%)
  local copies, waits for them, and re-layouts  5.09 us (2%)
    all_gather x1, waiting for transfers between devices, body(): piece_cols = lax.all_gather(arrived, 'tp', axis=2, tiled=True)  98.1 us
    all_gather x1, waiting for transfers between devices, body(): lax.all_gather(hidden, 'tp', axis=1, tiled=True)  67.7 us
    all_to_all x1, blocking collectives, from_everyone(): lax.all_to_all(jnp.broadcast_to(value[None], (length, *value.shape)), axi...  21.2 us
    all_to_all x1, blocking collectives, body(): lax.all_to_all(outgoing, 'ep', split_axis=1, concat_axis=1, tiled=True)  14.9 us
    all_to_all x1, waiting for transfers between devices, body(): lax.all_to_all(expert_out.reshape(EXP_DEV, ep_count, slot_count, out_part...  8.16 us
    all_to_all x1, starting transfers between devices, body(): lax.all_to_all(expert_out.reshape(EXP_DEV, ep_count, slot_count, out_part...  6.53 us
    dot_general x1, other arithmetic, body(): jnp.einsum('esn,esn->es', piece_cols, piece_cols, preferred_element_type=...  5.23 us
  transfers between devices with their start and end apart: 3, of which 3 were waited for; matrix products, arithmetic and copies ran while one was open for 0% of the time, Pallas kernels for 0%

commit v1 on v0

--- a/solution.py
+++ b/solution.py
@@ -1,3 +1,4 @@
+import functools
 import jax
 import jax.numpy as jnp
 from jax import lax
@@ -7,6 +8,21 @@
 TOPK = 4
 EXP_DEV = 2
 norm_eps = 1e-05
+
+
+def _place_levels_all(point, net_axis):
+    return jnp.concatenate(
+        lax.all_to_all(
+            jnp.stack([point for _ in range(lax.axis_size(net_axis))]),
+            concat_axis=0,
+            axis_name=net_axis,
+            split_axis=0,
+        ),
+        axis=2,
+    )
+
+
+seats_all_work = functools.partial(_place_levels_all, net_axis="tp")
 
 
 def from_everyone(value, axis):
@@ -46,7 +62,7 @@
     arrived = lax.all_to_all(outgoing, "ep", split_axis=1, concat_axis=1, tiled=True).reshape(
         EXP_DEV, span_rows, width_part
     )
-    piece_cols = lax.all_gather(arrived, "tp", axis=2, tiled=True)
+    piece_cols = seats_all_work(arrived)
     gate_sum = jnp.einsum("efn,esn->efs", w_gate, piece_cols, preferred_element_type=jnp.float32)
     up_sum = jnp.einsum("efn,esn->efs", w_up, piece_cols, preferred_element_type=jnp.float32)
     square_sum = jnp.einsum(

time: 254 us -> 532 us (2.09)
  blocking collectives: 36.1 us -> 424 us
  waiting for transfers between devices: 174 us -> 67.8 us
    all_to_all x0 -> x1, blocking collectives: none -> 387 us  [_place_levels_all(): lax.all_to_all(jnp.stack([point for _ in range(lax.axis_size(net_axis))])...]
    all_gather x1 -> x0, waiting for transfers between devices: 98.1 us -> none  [body(): piece_cols = lax.all_gather(arrived, 'tp', axis=2, tiled=True)]
    all_gather x1, waiting for transfers between devices: 67.7 us -> 59.6 us  [body(): lax.all_gather(hidden, 'tp', axis=1, tiled=True)]
  transfers between devices with their start and end apart: 3 -> 2, of which waited for: 3 -> 2; matrix products, arithmetic and copies ran while one was open for 0% -> 0% of each run, Pallas kernels for 0% -> 0%
where the time goes in v1:
time: 532 us
  blocking collectives  424 us (80%)
  waiting for transfers between devices  67.8 us (13%)
  between operations  13.5 us (3%)
  matrix products  9.17 us (2%)
  starting transfers between devices  6.53 us (1%)
  local copies, waits for them, and re-layouts  5.87 us (1%)
    all_to_all x1, blocking collectives, _place_levels_all(): lax.all_to_all(jnp.stack([point for _ in range(lax.axis_size(net_axis))])...  387 us
    all_gather x1, waiting for transfers between devices, body(): lax.all_gather(hidden, 'tp', axis=1, tiled=True)  59.6 us
    all_to_all x1, blocking collectives, from_everyone(): lax.all_to_all(jnp.broadcast_to(value[None], (length, *value.shape)), axi...  21.2 us
    all_to_all x1, blocking collectives, body(): lax.all_to_all(outgoing, 'ep', split_axis=1, concat_axis=1, tiled=True)  14.9 us
  transfers between devices with their start and end apart: 2, of which 2 were waited for; matrix products, arithmetic and copies ran while one was open for 0% of the time, Pallas kernels for 0%

profile of v1, /device:TPU:1, one launch (start us, length us, event | category | flops | bytes accessed | tf_op | source)
XLA Modules:
  0.0 531.7 jit_solution(17995308172807580456)
XLA Ops:
  6.5 0.0 copy-start
  6.5 0.0 all-gather.2.cloned.1.call-start
  6.5 0.8 copy.92
  7.4 0.1 eq.44
  7.5 0.1 eq.40
  7.6 1.2 reduce-window.6
  8.8 0.2 slice_reduce_fusion
  9.0 0.1 fusion.29
  9.2 0.1 reduce_sum.41
  9.3 0.1 copy.95
  9.3 0.7 fusion.33
  10.1 0.4 fusion.7
  10.4 1.0 convolution_convert_fusion.1
  11.4 14.9 %all_to_all.21 = bf16[2,16,32,128]{3,2,0,1:T(8,128)(2,1)S(1)} all-to-all(bf16[2,16,32,128]{3,2,0,1:T(8,128)(2,1)S(1)} %copy.96), channel_id=1, replica_groups=mesh['ep'=16,'tp'=32] {'ep'}, dimensions={1} | all-to-all | bytes 524288 | tf_op jit(solution)/shard_map/all_to_all | solution.py:62
  26.4 2.0 stack.3
  28.4 387.4 %all_to_all.22 = bf16[32,2,512,128]{3,2,1,0:T(8,128)(2,1)S(1)} all-to-all(bf16[32,2,512,128]{3,2,1,0:T(8,128)(2,1)S(1)} %stack.3), channel_id=1, replica_groups=mesh['ep'=16,'tp'=32] {'tp'}, dimensions={0} | all-to-all | bytes 16777216 | tf_op jit(solution)/shard_map/all_to_all | solution.py:15
  415.8 0.0 copy-start.3
  415.8 0.0 copy-start.4
  415.8 1.7 fusion
  417.6 0.0 copy-done.3
  417.6 2.5 fusion.11
  420.1 0.0 copy-done.4
  420.1 0.0 copy-start.1
  420.1 0.0 copy-start.2
  420.1 3.2 fusion.23
  423.3 0.0 all-gather.2.cloned.1.call-update
  423.3 0.1 reshape.215
  423.4 0.0 copy-done.1
  423.4 0.1 copy.102
  423.6 59.6 %all-gather.2.cloned.1.call-done = bf16[2,1024,512]{2,1,0:T(8,128)(2,1)} async-done(((bf16[2,32,512]{2,1,0:T(8,128)(2,1)}), bf16[2,1024,512]{2,1,0:T(8,128)(2,1)}) %all-gather.2.cloned.1.call-update) | async-done | bytes 2097168 | tf_op jit(solution)/shard_map/all_gather | solution.py:76
  483.2 0.0 copy-done
  483.2 2.5 convolution_convert_fusion
  485.7 0.7 copy.99
  486.4 6.5 %all-to-all-start.2 = ((bf16[2,16,32,128]{3,2,0,1:T(8,128)(2,1)}), bf16[2,16,32,128]{3,2,0,1:T(8,128)(2,1)S(1)}, u32[]{:S(2)}, u32[]{:S(2)}) async-start(bf16[2,16,32,128]{3,2,0,1:T(8,128)(2,1)} %copy.99), calls=%async_computation.2 | async-start | bytes 524288 | tf_op jit(solution)/shard_map/all_to_all | solution.py:80
  493.0 8.2 %all-to-all-done.2 = bf16[2,16,32,128]{3,2,0,1:T(8,128)(2,1)S(1)} async-done(((bf16[2,16,32,128]{3,2,0,1:T(8,128)(2,1)}), bf16[2,16,32,128]{3,2,0,1:T(8,128)(2,1)S(1)}, u32[]{:S(2)}, u32[]{:S(2)}) %all-to-all-start.2) | async-done | bytes 262176 | tf_op jit(solution)/shard_map/all_to_all | solution.py:80
  501.2 1.3 gather_fusion
  502.5 0.2 fusion.26
  502.8 0.1 multiply_reduce_fusion
  502.9 21.2 %all_to_all.23 = f32[32,1,128]{2,1,0:T(1,128)S(1)} all-to-all(f32[32,1,128]{2,1,0:T(1,128)S(1)} %broadcast_in_dim.2), channel_id=1, replica_groups=mesh['ep'=16,'tp'=32] {'tp'}, dimensions={0} | all-to-all | bytes 32768 | tf_op jit(solution)/shard_map/all_to_all | solution.py:30
  524.1 0.0 copy-done.2
  524.1 0.7 multiply_convert_fusion
  (12 shorter events, 0.2 us)
Async XLA Ops:
  6.5 476.6 %copy-start = (bf16[2,1024,128]{2,1,0:T(8,128)(2,1)S(1)}, bf16[2,1024,128]{2,1,0:T(8,128)(2,1)}, u32[]{:S(2)}) copy-start(bf16[2,1024,128]{2,1,0:T(8,128)(2,1)} %param.12) | copy-start | bytes 1572868
  6.5 476.6 %all-gather.2.cloned.1.call-start = ((), (), s32[]{:S(2)}) async-start(), calls=%async_computation.4 | async-start | bytes 2162688 | tf_op jit(solution)/shard_map/all_gather | solution.py:76
  415.8 1.7 copy-start.3
  415.8 4.3 copy-start.4
  420.1 3.3 copy-start.1
  420.1 104.0 %copy-start.2 = (f32[128]{0:T(128)S(1)}, f32[128]{0:T(128)}, u32[]{:S(2)}) copy-start(f32[128]{0:T(128)} %param.13) | copy-start | bytes 1540
  486.4 14.7 %all-to-all-start.2 = ((bf16[2,16,32,128]{3,2,0,1:T(8,128)(2,1)}), bf16[2,16,32,128]{3,2,0,1:T(8,128)(2,1)S(1)}, u32[]{:S(2)}, u32[]{:S(2)}) async-start(bf16[2,16,32,128]{3,2,0,1:T(8,128)(2,1)} %copy.99), calls=%async_computation.2 | async-start | bytes 524288 | tf_op jit(solution)/shard_map/all_to_all | solution.py:80
Sparse Core Ops, SparseCore 0:
  423.4 59.6 all-gather.1
